TPU v7x, 32 devices: a whole 2x2x4 slice. The times are simulated.
32 devices in a mesh: rep: 4 (over z), fs: 2 (over y), tp: 4 (over x, core).
Axes of the slice: x: 2, y: 2, z: 4, core: 2. Of those that a mesh axis runs over, the one named last changes fastest.
Arguments:
- inputs: bfloat16 [512, 4096], P('rep'), may hold values from -6 to 6
- cotangent: bfloat16 [512, 4096], P('rep'), may hold values from -6 to 6
- w_gate: bfloat16 [4096, 11264], P(None, ('fs', 'tp')), may hold values from -0.09375 to 0.09375
- w_upward: bfloat16 [4096, 11264], P(None, ('fs', 'tp')), may hold values from -0.09375 to 0.09375
- w_down: bfloat16 [11264, 4096], P(('fs', 'tp')), may hold values from -0.0546875 to 0.0546875
Outputs:
- grad_input: bfloat16 [512, 4096], P('rep')
- grad_gate: float32 [4096, 11264], P('rep', ('fs', 'tp'))
- grad_upward: float32 [4096, 11264], P('rep', ('fs', 'tp'))
- grad_down: float32 [11264, 4096], P(('fs', 'tp'), 'rep')
All inputs are finite; a program needn't handle non-finite values.
Results may differ from a plain program's by a relative error of at most 0.0049.
Values may be sent and summed in bfloat16 or wider, within the bound.
A program may use at most 128 MiB of HBM per device.

v0:
```python
import jax
import jax.numpy as jnp
from jax import lax
from jax.sharding import PartitionSpec as P


def contract_rows(left, right):
    return lax.dot_general(
        left, right, (((0,), (0,)), ((), ())), preferred_element_type=jnp.float32
    )


def contract_cols(left, right):
    return lax.dot_general(
        left, right, (((1,), (1,)), ((), ())), preferred_element_type=jnp.float32
    )


def local(inputs, cotangent, w_gate, w_upward, w_down):
    gate_pre = jnp.dot(inputs, w_gate, preferred_element_type=jnp.float32)
    up_pre = jnp.dot(inputs, w_upward, preferred_element_type=jnp.float32)
    sigmoid_gate = jax.nn.sigmoid(gate_pre)
    activated = gate_pre * sigmoid_gate
    hidden = (activated * up_pre).astype(jnp.bfloat16)
    hidden_grad = contract_cols(cotangent, w_down)
    gate_delta = (
        hidden_grad * up_pre * sigmoid_gate * (1.0 + gate_pre * (1.0 - sigmoid_gate))
    ).astype(jnp.bfloat16)
    up_delta = (hidden_grad * activated).astype(jnp.bfloat16)
    input_cols, cotangent_cols = (
        lax.all_to_all(inputs, "rep", split_axis=1, concat_axis=0, tiled=True),
        lax.all_to_all(cotangent, "rep", split_axis=1, concat_axis=0, tiled=True),
    )
    piece_gate = lax.all_gather(gate_delta, "rep", axis=0, tiled=True)
    piece_up = lax.all_gather(up_delta, "rep", axis=0, tiled=True)
    piece_hidden = lax.all_gather(hidden, "rep", axis=0, tiled=True)
    grad_gate = contract_rows(input_cols, piece_gate)
    grad_upward = contract_rows(input_cols, piece_up)
    grad_down = contract_rows(piece_hidden, cotangent_cols)
    input_terms = contract_cols(gate_delta, w_gate) + contract_cols(up_delta, w_upward)
    grad_input = lax.psum(input_terms, ("fs", "tp")).astype(jnp.bfloat16)
    return (grad_input, grad_gate, grad_upward, grad_down)


def solution(mesh):
    in_specs = (
        P("rep", None),
        P("rep", None),
        P(None, ("fs", "tp")),
        P(None, ("fs", "tp")),
        P(("fs", "tp"), None),
    )
    out_specs = (
        P("rep", None),
        P("rep", ("fs", "tp")),
        P("rep", ("fs", "tp")),
        P(("fs", "tp"), "rep"),
    )
    return jax.shard_map(local, mesh=mesh, in_specs=in_specs, out_specs=out_specs, check_vma=False)
```

profile of v0, /device:TPU:0, one launch (start us, length us, event | category | flops | bytes accessed | tf_op | source)
XLA Modules:
  0.0 190.2 jit_solution(5874101361756558968)
XLA Ops:
  7.2 0.0 all-gather.4.cloned.1.call-start
  7.2 8.6 %fusion.1 = f32[128,1408]{1,0:T(8,128)S(1)} fusion(bf16[128,4096]{1,0:T(8,128)(2,1)} %param.6, bf16[1408,4096]{1,0:T(8,128)(2,1)} %param.9), kind=kOutput, calls=%fused_computation.8 | convolution fusion | flops 1476395008 | bytes 13303808 | tf_op jit(solution)/shard_map/dot_general | solution.py:14
  15.8 1.8 fusion.2
  17.7 2.4 %copy-done.1 = bf16[4096,1408]{1,0:T(8,128)(2,1)S(1)} copy-done((bf16[4096,1408]{1,0:T(8,128)(2,1)S(1)}, bf16[4096,1408]{1,0:T(8,128)(2,1)}, u32[]{:S(2)}) %copy-start.1) | copy-done | bytes 11534360
  20.1 3.0 %multiply_convert_fusion = (bf16[128,1408]{1,0:T(8,128)(2,1)}, bf16[128,1408]{1,0:T(8,128)(2,1)}, bf16[128,1408]{1,0:T(8,128)(2,1)}) fusion(f32[128,1408]{1,0:T(8,128)S(1)} %fusion.2, f32[128,1408]{1,0:T(8,128)S(1)} %fusion.1, bf16[128,4096]{1,0:T(8,128)(2,1)S(1)} %copy-done.2, bf16[4096,1408]{1,0:T(8,128)(2,1)S(1)} %copy-done.1), kind=kOutput, calls=%fused_computation.3 | convolution fusion | flops 1479098368 | bytes 15106048 | tf_op jit(solution)/shard_map/dot_general | solution.py:21
  23.1 0.0 all-gather.6.cloned.1.call-start
  23.2 0.7 all-gather.6.cloned.1.call-update
  23.9 1.3 copy.13
  25.2 6.3 %all-to-all-start = ((bf16[128,4,1024]{0,2,1:T(8,128)(2,1)}), bf16[128,4,1024]{0,2,1:T(8,128)(2,1)S(1)}, u32[]{:S(2)}, u32[]{:S(2)}) async-start(bf16[128,4,1024]{0,2,1:T(8,128)(2,1)} %bitcast.27), calls=%async_computation | async-start | bytes 2097152 | tf_op jit(solution)/shard_map/all_to_all | solution.py:31
  31.5 0.7 all-gather.8.cloned.1.call-update
  32.3 1.3 copy.15
  33.6 9.5 %fusion.3 = f32[128,4096]{1,0:T(8,128)} fusion(bf16[128,1408]{1,0:T(8,128)(2,1)S(1)} %copy-done.4, bf16[4096,1408]{1,0:T(8,128)(2,1)} %param.7), kind=kOutput, calls=%fused_computation.10 | convolution fusion | flops 1476395008 | bytes 13991936 | tf_op jit(solution)/shard_map/dot_general | solution.py:14
  43.1 37.0 %all-to-all-done = bf16[128,4,1024]{0,2,1:T(8,128)(2,1)S(1)} async-done(((bf16[128,4,1024]{0,2,1:T(8,128)(2,1)}), bf16[128,4,1024]{0,2,1:T(8,128)(2,1)S(1)}, u32[]{:S(2)}, u32[]{:S(2)}) %all-to-all-start) | async-done | bytes 1048608 | tf_op jit(solution)/shard_map/all_to_all | solution.py:31
  80.1 4.3 %all-to-all-start.1 = ((bf16[128,4,1024]{0,2,1:T(8,128)(2,1)}), bf16[128,4,1024]{0,2,1:T(8,128)(2,1)}, u32[]{:S(2)}, u32[]{:S(2)}) async-start(bf16[128,4,1024]{0,2,1:T(8,128)(2,1)} %bitcast.5), calls=%async_computation.1 | async-start | bytes 2097152 | tf_op jit(solution)/shard_map/all_to_all | solution.py:32
  84.3 9.0 %convolution_add_fusion = f32[128,4096]{1,0:T(8,128)S(1)} fusion(f32[128,4096]{1,0:T(8,128)} %fusion.3, bf16[128,1408]{1,0:T(8,128)(2,1)} %get-tuple-element.18, bf16[4096,1408]{1,0:T(8,128)(2,1)} %param.8), kind=kOutput, calls=%fused_computation | convolution fusion | flops 1476919296 | bytes 16089088 | tf_op jit(solution)/shard_map/dot_general | solution.py:14
  93.3 59.1 %all-reduce.1 = bf16[128,4096]{1,0:T(8,128)(2,1)} all-reduce(f32[128,4096]{1,0:T(8,128)S(1)} %convolution_add_fusion), channel_id=1, replica_groups=mesh['rep'=4,'fs'=2,'tp'=4] {'fs','tp'}, use_global_device_ids=true, to_apply=%region_0.0 | all-reduce | flops 524288 | bytes 3145728 | tf_op jit(solution)/shard_map/psum | solution.py:41
  152.4 0.5 copy.14
  153.0 1.5 copy.16
  154.5 0.0 all-gather.4.cloned.1.call-done
  154.5 5.6 %convolution_bitcast_fusion.1 = f32[1024,1408]{0,1:T(8,128)} fusion(bf16[512,1408]{1,0:T(8,128)(2,1)} %all-gather.4.cloned.1.call-done, bf16[512,1024]{1,0:T(8,128)(2,1)S(1)} %bitcast.29), kind=kOutput, calls=%fused_computation.2 | convolution fusion | flops 1476395008 | bytes 8257536 | tf_op jit(solution)/shard_map/dot_general | solution.py:8
  160.1 6.2 %copy.17 = f32[1024,1408]{1,0:T(8,128)} copy(f32[1024,1408]{0,1:T(8,128)} %convolution_bitcast_fusion.1) | data formatting | bytes 11534336
  166.3 5.6 %convolution_bitcast_fusion = f32[1024,1408]{0,1:T(8,128)} fusion(bf16[512,1408]{1,0:T(8,128)(2,1)} %all-gather.6.cloned.1.call-done, bf16[512,1024]{1,0:T(8,128)(2,1)S(1)} %bitcast.30), kind=kOutput, calls=%fused_computation.1 | convolution fusion | flops 1476395008 | bytes 8257536 | tf_op jit(solution)/shard_map/dot_general | solution.py:8
  171.9 6.2 %copy.18 = f32[1024,1408]{1,0:T(8,128)} copy(f32[1024,1408]{0,1:T(8,128)} %convolution_bitcast_fusion) | data formatting | bytes 11534336
  178.1 5.6 %fusion.4 = f32[1408,1024]{1,0:T(8,128)} fusion(bf16[512,1408]{1,0:T(8,128)(2,1)} %all-gather.8.cloned.1.call-done, bf16[512,1024]{1,0:T(8,128)(2,1)S(1)} %bitcast.28), kind=kOutput, calls=%fused_computation.11 | convolution fusion | flops 1476395008 | bytes 8257536 | tf_op jit(solution)/shard_map/dot_general | solution.py:8
  (14 shorter events, 0.0 us)
Async XLA Ops:
  7.2 8.6 %copy-start.2 = (bf16[128,4096]{1,0:T(8,128)(2,1)S(1)}, bf16[128,4096]{1,0:T(8,128)(2,1)}, u32[]{:S(2)}) copy-start(bf16[128,4096]{1,0:T(8,128)(2,1)} %param.5) | copy-start | bytes 3145732
  7.2 147.3 %all-gather.4.cloned.1.call-start = ((), (), s32[]{:S(2)}) async-start(), calls=%async_computation.2 | async-start | bytes 1802240 | tf_op jit(solution)/shard_map/all_gather | solution.py:34
  7.2 8.6 %copy-start = (bf16[4096,1408]{1,0:T(8,128)(2,1)S(1)}, bf16[4096,1408]{1,0:T(8,128)(2,1)}, u32[]{:S(2)}) copy-start(bf16[4096,1408]{1,0:T(8,128)(2,1)} %param.7) | copy-start | bytes 34603012
  15.8 4.3 %copy-start.1 = (bf16[4096,1408]{1,0:T(8,128)(2,1)S(1)}, bf16[4096,1408]{1,0:T(8,128)(2,1)}, u32[]{:S(2)}) copy-start(bf16[4096,1408]{1,0:T(8,128)(2,1)} %param.8) | copy-start | bytes 34603012
  23.1 9.2 %copy-start.3 = (bf16[128,4096]{1,0:T(8,128)(2,1)S(1)}, bf16[128,4096]{1,0:T(8,128)(2,1)}, u32[]{:S(2)}) copy-start(bf16[128,4096]{1,0:T(8,128)(2,1)} %param.6) | copy-start | bytes 3145732
  23.1 10.5 %copy-start.4 = (bf16[128,1408]{1,0:T(8,128)(2,1)S(1)}, bf16[128,1408]{1,0:T(8,128)(2,1)}, u32[]{:S(2)}) copy-start(bf16[128,1408]{1,0:T(8,128)(2,1)} %get-tuple-element.17) | copy-start | bytes 1081348
  23.1 143.2 %all-gather.6.cloned.1.call-start = ((), (), s32[]{:S(2)}) async-start(), calls=%async_computation.3 | async-start | bytes 1802240 | tf_op jit(solution)/shard_map/all_gather | solution.py:35
  25.2 54.9 %all-to-all-start = ((bf16[128,4,1024]{0,2,1:T(8,128)(2,1)}), bf16[128,4,1024]{0,2,1:T(8,128)(2,1)S(1)}, u32[]{:S(2)}, u32[]{:S(2)}) async-start(bf16[128,4,1024]{0,2,1:T(8,128)(2,1)} %bitcast.27), calls=%async_computation | async-start | bytes 2097152 | tf_op jit(solution)/shard_map/all_to_all | solution.py:31
  31.5 146.6 %all-gather.8.cloned.1.call-start = ((), (), s32[]{:S(2)}) async-start(), calls=%async_computation.4 | async-start | bytes 1802240 | tf_op jit(solution)/shard_map/all_gather | solution.py:36
  80.1 72.9 %all-to-all-start.1 = ((bf16[128,4,1024]{0,2,1:T(8,128)(2,1)}), bf16[128,4,1024]{0,2,1:T(8,128)(2,1)}, u32[]{:S(2)}, u32[]{:S(2)}) async-start(bf16[128,4,1024]{0,2,1:T(8,128)(2,1)} %bitcast.5), calls=%async_computation.1 | async-start | bytes 2097152 | tf_op jit(solution)/shard_map/all_to_all | solution.py:32
Sparse Core Ops, SparseCore 0:
  23.2 57.4 all-gather.3
  82.3 48.3 all-gather.5
  132.3 33.8 all-gather.7
where the time goes:
time: 191 us; the launch traced here: 190 us
  blocking collectives  59.1 us (31%)
  matrix products  48.6 us (25%)
  waiting for transfers between devices  38.5 us (20%)
  local copies, waits for them, and re-layouts  19.5 us (10%)
  between operations  13.9 us (7%)
  starting transfers between devices  10.7 us (6%)
    psum x1, blocking collectives, local(): grad_input = lax.psum(input_terms, ('fs', 'tp')).astype(jnp.bfloat16)  59.1 us
    all_to_all x1, waiting for transfers between devices, local(): lax.all_to_all(inputs, 'rep', split_axis=1, concat_axis=0, tiled=True)  37 us
    dot_general x3, matrix products, contract_cols(): lax.dot_general(left, right, (((1,), (1,)), ((), ())), preferred_element_...  27 us
    unnamed x14, local copies, waits for them, and re-layouts  17.5 us
    dot_general x3, matrix products, contract_rows(): lax.dot_general(left, right, (((0,), (0,)), ((), ())), preferred_element_...  16.7 us
    all_to_all x1, starting transfers between devices, local(): lax.all_to_all(inputs, 'rep', split_axis=1, concat_axis=0, tiled=True)  6.35 us
    all_to_all x1, starting transfers between devices, local(): lax.all_to_all(cotangent, 'rep', split_axis=1, concat_axis=0, tiled=True)  4.27 us
  transfers between devices with their start and end apart: 5, of which 1 were waited for; matrix products, arithmetic and copies ran while one was open for 25% of the time, Pallas kernels for 0%

commit v1 on v0

v1 whole, which is shorter than its diff:
```python
import jax
import jax.numpy as jnp
from jax import lax
from jax.sharding import PartitionSpec as P

PLANE = ("fs", "tp")


def contract_rows(left, right):
    return lax.dot_general(
        left, right, (((0,), (0,)), ((), ())), preferred_element_type=jnp.float32
    )


def contract_cols(left, right):
    return lax.dot_general(
        left, right, (((1,), (1,)), ((), ())), preferred_element_type=jnp.float32
    )


def forward(inputs, cotangent, w_gate, w_upward, w_down):
    gate_pre = jnp.dot(inputs, w_gate, preferred_element_type=jnp.float32)
    up_pre = jnp.dot(inputs, w_upward, preferred_element_type=jnp.float32)
    sigmoid_gate = jax.nn.sigmoid(gate_pre)
    activated = gate_pre * sigmoid_gate
    hidden = (activated * up_pre).astype(jnp.bfloat16)
    hidden_grad = contract_cols(cotangent, w_down)
    gate_delta = (
        hidden_grad * up_pre * sigmoid_gate * (1.0 + gate_pre * (1.0 - sigmoid_gate))
    ).astype(jnp.bfloat16)
    up_delta = (hidden_grad * activated).astype(jnp.bfloat16)
    return gate_delta, up_delta, hidden


def local(planes, inputs, cotangent, w_gate, w_upward, w_down):
    rows, width = inputs.shape
    share = rows // planes
    me = lax.axis_index(PLANE)
    mine = [lax.dynamic_slice_in_dim(a, me * share, share, 0) for a in (inputs, cotangent)]
    everyone = ("rep",) + PLANE
    all_inputs, all_cotangent = [lax.all_gather(a, everyone, axis=0, tiled=True) for a in mine]

    gate_delta, up_delta, _ = forward(inputs, cotangent, w_gate, w_upward, w_down)
    terms = contract_cols(gate_delta, w_gate) + contract_cols(up_delta, w_upward)
    terms = terms.astype(jnp.bfloat16)
    terms = lax.all_to_all(terms.reshape(planes, share, width), PLANE, 0, 0)
    total = jnp.sum(terms.astype(jnp.float32), axis=0).astype(jnp.bfloat16)
    grad_input = lax.all_gather(total, PLANE, axis=0, tiled=True)

    gate_delta, up_delta, hidden = forward(all_inputs, all_cotangent, w_gate, w_upward, w_down)
    reps = all_inputs.shape[0] // rows
    cols = width // reps
    at = lax.axis_index("rep") * cols
    input_cols = lax.dynamic_slice_in_dim(all_inputs, at, cols, 1)
    cotangent_cols = lax.dynamic_slice_in_dim(all_cotangent, at, cols, 1)
    grad_gate = contract_rows(input_cols, gate_delta)
    grad_upward = contract_rows(input_cols, up_delta)
    grad_down = contract_rows(hidden, cotangent_cols)
    return (grad_input, grad_gate, grad_upward, grad_down)


def solution(mesh):
    planes = mesh.shape["fs"] * mesh.shape["tp"]
    in_specs = (
        P("rep", None),
        P("rep", None),
        P(None, PLANE),
        P(None, PLANE),
        P(PLANE, None),
    )
    out_specs = (
        P("rep", None),
        P("rep", PLANE),
        P("rep", PLANE),
        P(PLANE, "rep"),
    )

    def body(*args):
        return local(planes, *args)

    return jax.shard_map(body, mesh=mesh, in_specs=in_specs, out_specs=out_specs, check_vma=False)
```

time: 191 us -> 249 us (1.30)
  waiting for transfers between devices: 38.5 us -> 125 us
  blocking collectives: 59.1 us -> 20.3 us
  matrix products: 48.6 us -> 84.8 us
  local copies, waits for them, and re-layouts: 19.5 us -> 3.26 us
  starting transfers between devices: 10.7 us -> 0.3 us
    all_gather x3, waiting for transfers between devices: 0.02 us -> 125 us  [the longest x2 105 us: local(): lax.all_gather(a, everyone, axis=0, tiled=True)]
    psum x1 -> x0, blocking collectives: 59.1 us -> none  [local(): grad_input = lax.psum(input_terms, ('fs', 'tp')).astype(jnp.bfloat16)]
    all_to_all x2 -> x0, waiting for transfers between devices: 37 us -> none  [the longest x1 37 us: local(): lax.all_to_all(inputs, 'rep', split_axis=1, concat_axis=0, tiled=True)]
    dot_general x2 -> x3, matrix products: 4.82 us -> 27 us  [the longest x2 15.9 us: forward(): gate_pre = jnp.dot(inputs, w_gate, preferred_element_type=jnp.float32)]
    all_to_all x0 -> x1, blocking collectives: none -> 20.3 us  [local(): terms = lax.all_to_all(terms.reshape(planes, share, width), PLANE, 0, 0)]
    unnamed x14 -> x17, local copies, waits for them, and re-layouts: 17.5 us -> 1.01 us
    dot_general x3 -> x4, matrix products: 27 us -> 43 us  [contract_cols(): lax.dot_general(left, right, (((1,), (1,)), ((), ())), preferred_element_...]
    all_to_all x2 -> x0, starting transfers between devices: 10.6 us -> none  [the longest x1 6.35 us: local(): lax.all_to_all(inputs, 'rep', split_axis=1, concat_axis=0, tiled=True)]
  transfers between devices with their start and end apart: 5 -> 3, of which waited for: 1 -> 3; matrix products, arithmetic and copies ran while one was open for 25% -> 11% of each run, Pallas kernels for 0% -> 0%
where the time goes in v1:
time: 249 us
  waiting for transfers between devices  125 us (50%)
  matrix products  84.8 us (34%)
  blocking collectives  20.3 us (8%)
  between operations  13.8 us (6%)
  local copies, waits for them, and re-layouts  3.26 us (1%)
    all_gather x2, waiting for transfers between devices, local(): lax.all_gather(a, everyone, axis=0, tiled=True)  105 us
    dot_general x4, matrix products, contract_cols(): lax.dot_general(left, right, (((1,), (1,)), ((), ())), preferred_element_...  43 us
    all_to_all x1, blocking collectives, local(): terms = lax.all_to_all(terms.reshape(planes, share, width), PLANE, 0, 0)  20.3 us
    all_gather x1, waiting for transfers between devices, local(): grad_input = lax.all_gather(total, PLANE, axis=0, tiled=True)  20.3 us
    dot_general x2, matrix products, forward(): gate_pre = jnp.dot(inputs, w_gate, preferred_element_type=jnp.float32)  15.9 us
    dot_general x3, matrix products, contract_rows(): lax.dot_general(left, right, (((0,), (0,)), ((), ())), preferred_element_...  14.8 us
    dot_general x1, matrix products, forward(): up_pre = jnp.dot(inputs, w_upward, preferred_element_type=jnp.float32)  11.1 us
  transfers between devices with their start and end apart: 3, of which 3 were waited for; matrix products, arithmetic and copies ran while one was open for 11% of the time, Pallas kernels for 0%

profile of v1, /device:TPU:0, one launch (start us, length us, event | category | flops | bytes accessed | tf_op | source)
XLA Modules:
  0.0 248.5 jit_solution(1418914118768218040)
XLA Ops:
  7.2 0.0 all-gather.4.cloned.1.call-start
  7.2 9.4 %fusion.24 = f32[128,1408]{1,0:T(8,128)} fusion(bf16[128,4096]{1,0:T(8,128)(2,1)} %param.6, bf16[1408,4096]{1,0:T(8,128)(2,1)} %param.9), kind=kOutput, calls=%fused_computation.32 | convolution fusion | flops 1476395008 | bytes 13303808 | tf_op jit(solution)/shard_map/dot_general | solution.py:16
  16.7 2.7 %fusion.25 = f32[128,1408]{1,0:T(8,128)} fusion(bf16[128,4096]{1,0:T(8,128)(2,1)S(1)} %copy-done, bf16[4096,1408]{1,0:T(8,128)(2,1)S(1)} %copy-done.2), kind=kOutput, calls=%fused_computation.33 | convolution fusion | flops 1476395008 | bytes 13303808 | tf_op jit(solution)/shard_map/dot_general | solution.py:22
  19.4 13.5 %fusion.11 = f32[128,4096]{1,0:T(8,128)S(1)} fusion(bf16[4096,1408]{1,0:T(8,128)(2,1)} %param.7, f32[128,1408]{1,0:T(8,128)} %fusion.24, bf16[128,4096]{1,0:T(8,128)(2,1)S(1)} %copy-done, bf16[4096,1408]{1,0:T(8,128)(2,1)} %param.8, f32[128,1408]{1,0:T(8,128)} %fusion.25), kind=kOutput, calls=%fused_computation.19 | convolution fusion | flops 2954592256 | bytes 27656192 | tf_op jit(solution)/shard_map/dot_general | solution.py:16
  32.9 8.5 %fusion = bf16[128,4096]{1,0:T(8,128)(2,1)S(1)} fusion(f32[128,4096]{1,0:T(8,128)S(1)} %fusion.11, bf16[4096,1408]{1,0:T(8,128)(2,1)} %param.8, f32[128,1408]{1,0:T(8,128)} %fusion.24, f32[128,1408]{1,0:T(8,128)} %fusion.25), kind=kOutput, calls=%fused_computation.1 | convolution fusion | flops 1478524928 | bytes 16121856 | tf_op jit(solution)/shard_map/dot_general | solution.py:16
  41.5 20.3 %all_to_all.5 = bf16[8,16,4096]{2,1,0:T(8,128)(2,1)S(1)} all-to-all(bf16[8,16,4096]{2,1,0:T(8,128)(2,1)S(1)} %bitcast.15), channel_id=1, replica_groups=mesh['rep'=4,'fs'=2,'tp'=4] {'fs','tp'}, dimensions={0} | all-to-all | bytes 2097152 | tf_op jit(solution)/shard_map/all_to_all | solution.py:46
  61.8 0.8 reduce_sum.12
  62.6 0.0 all-gather.4.cloned.1.call-update
  62.6 0.0 all-gather.6.cloned.1.call-start
  62.7 0.7 constant_dynamic-slice_fusion.1
  63.4 0.0 all-gather.6.cloned.1.call-update
  63.4 0.2 all-gather.8.cloned.1.call-start
  63.6 1.6 constant_dynamic-slice_fusion
  65.2 0.0 all-gather.8.cloned.1.call-update
  65.2 20.3 %all-gather.4.cloned.1.call-done = bf16[128,4096]{1,0:T(8,128)(2,1)} async-done(((bf16[16,4096]{1,0:T(8,128)(2,1)}), bf16[128,4096]{1,0:T(8,128)(2,1)}) %all-gather.4.cloned.1.call-update) | async-done | bytes 1048592 | tf_op jit(solution)/shard_map/all_gather | solution.py:48
  85.5 65.2 %all-gather.6.cloned.1.call-done = bf16[512,4096]{1,0:T(8,128)(2,1)} async-done(((bf16[16,4096]{1,0:T(8,128)(2,1)}), bf16[512,4096]{1,0:T(8,128)(2,1)}) %all-gather.6.cloned.1.call-update) | async-done | bytes 4194320 | tf_op jit(solution)/shard_map/all_gather | solution.py:41
  150.7 13.2 %fusion.28 = f32[512,1408]{1,0:T(8,128)} fusion(bf16[512,4096]{1,0:T(8,128)(2,1)} %all-gather.6.cloned.1.call-done, bf16[4096,1408]{1,0:T(8,128)(2,1)} %param.7), kind=kOutput, calls=%fused_computation.36 | convolution fusion | flops 5905580032 | bytes 18612224 | tf_op jit(solution)/shard_map/dot_general | solution.py:22
  163.9 11.1 %fusion.27 = f32[512,1408]{1,0:T(8,128)} fusion(bf16[512,4096]{1,0:T(8,128)(2,1)S(1)} %copy-done.4, bf16[4096,1408]{1,0:T(8,128)(2,1)} %param.8), kind=kOutput, calls=%fused_computation.35 | convolution fusion | flops 5905580032 | bytes 18612224 | tf_op jit(solution)/shard_map/dot_general | solution.py:23
  175.0 39.7 %all-gather.8.cloned.1.call-done = bf16[512,4096]{1,0:T(8,128)(2,1)} async-done(((bf16[16,4096]{1,0:T(8,128)(2,1)}), bf16[512,4096]{1,0:T(8,128)(2,1)}) %all-gather.8.cloned.1.call-update) | async-done | bytes 4194320 | tf_op jit(solution)/shard_map/all_gather | solution.py:41
  214.7 11.5 %fusion.26 = f32[512,1408]{1,0:T(8,128)S(1)} fusion(bf16[512,4096]{1,0:T(8,128)(2,1)} %all-gather.8.cloned.1.call-done, bf16[1408,4096]{1,0:T(8,128)(2,1)} %param.9), kind=kOutput, calls=%fused_computation.34 | convolution fusion | flops 5905580032 | bytes 18612224 | tf_op jit(solution)/shard_map/dot_general | solution.py:16
  226.2 5.7 %fusion.6 = f32[1408,1024]{1,0:T(8,128)} fusion(f32[512,1408]{1,0:T(8,128)S(1)} %copy-done.7, bf16[512,4096]{1,0:T(8,128)(2,1)} %all-gather.8.cloned.1.call-done, s32[]{:T(128)S(6)} %select_n.9, f32[512,1408]{1,0:T(8,128)S(1)} %copy-done.6), kind=kOutput, calls=%fused_computation.12 | convolution fusion | flops 1480720384 | bytes 12582916 | tf_op jit(solution)/shard_map/dot_general | solution.py:10
  231.9 4.6 %fusion.7 = f32[1024,1408]{1,0:T(8,128)} fusion(f32[512,1408]{1,0:T(8,128)S(1)} %copy-done.6, f32[512,1408]{1,0:T(8,128)S(1)} %fusion.26, f32[512,1408]{1,0:T(8,128)S(1)} %copy-done.7, bf16[512,4096]{1,0:T(8,128)(2,1)S(1)} %copy-done.5, s32[]{:T(128)S(6)} %select_n.9), kind=kOutput, calls=%fused_computation.13 | convolution fusion | flops 1483603968 | bytes 15466500 | tf_op jit(solution)/shard_map/dot_general | solution.py:10
  236.5 4.5 %fusion.5 = f32[1024,1408]{1,0:T(8,128)} fusion(f32[512,1408]{1,0:T(8,128)S(1)} %fusion.26, bf16[512,4096]{1,0:T(8,128)(2,1)S(1)} %copy-done.5, s32[]{:T(128)S(6)} %select_n.9, f32[512,1408]{1,0:T(8,128)S(1)} %copy-done.6), kind=kOutput, calls=%fused_computation.11 | convolution fusion | flops 1480720384 | bytes 12582916 | tf_op jit(solution)/shard_map/dot_general | solution.py:10
  241.0 1.0 copy.10
  (16 shorter events, 0.0 us)
Async XLA Ops:
  7.2 9.5 %copy-start = (bf16[128,4096]{1,0:T(8,128)(2,1)S(1)}, bf16[128,4096]{1,0:T(8,128)(2,1)}, u32[]{:S(2)}) copy-start(bf16[128,4096]{1,0:T(8,128)(2,1)} %param.5) | copy-start | bytes 3145732
  7.2 78.3 %all-gather.4.cloned.1.call-start = ((), (), s32[]{:S(2)}) async-start(), calls=%async_computation.1 | async-start | bytes 1179648 | tf_op jit(solution)/shard_map/all_gather | solution.py:48
  7.2 9.4 %copy-start.2 = (bf16[4096,1408]{1,0:T(8,128)(2,1)S(1)}, bf16[4096,1408]{1,0:T(8,128)(2,1)}, u32[]{:S(2)}) copy-start(bf16[4096,1408]{1,0:T(8,128)(2,1)} %param.7) | copy-start | bytes 34603012
  62.6 88.1 %all-gather.6.cloned.1.call-start = ((), (), s32[]{:S(2)}) async-start(), calls=%async_computation.2 | async-start | bytes 4325376 | tf_op jit(solution)/shard_map/all_gather | solution.py:41
  63.4 151.3 %all-gather.8.cloned.1.call-start = ((), (), s32[]{:S(2)}) async-start(), calls=%async_computation.3 | async-start | bytes 4325376 | tf_op jit(solution)/shard_map/all_gather | solution.py:41
  150.7 13.2 %copy-start.4 = (bf16[512,4096]{1,0:T(8,128)(2,1)S(1)}, bf16[512,4096]{1,0:T(8,128)(2,1)}, u32[]{:S(2)}) copy-start(bf16[512,4096]{1,0:T(8,128)(2,1)} %all-gather.6.cloned.1.call-done) | copy-start | bytes 12582916
  214.7 11.5 %copy-start.6 = (f32[512,1408]{1,0:T(8,128)S(1)}, f32[512,1408]{1,0:T(8,128)}, u32[]{:S(2)}) copy-start(f32[512,1408]{1,0:T(8,128)} %fusion.28) | copy-start | bytes 8650756
  214.7 11.5 %copy-start.7 = (f32[512,1408]{1,0:T(8,128)S(1)}, f32[512,1408]{1,0:T(8,128)}, u32[]{:S(2)}) copy-start(f32[512,1408]{1,0:T(8,128)} %fusion.27) | copy-start | bytes 8650756
  226.2 5.7 %copy-start.5 = (bf16[512,4096]{1,0:T(8,128)(2,1)S(1)}, bf16[512,4096]{1,0:T(8,128)(2,1)}, u32[]{:S(2)}) copy-start(bf16[512,4096]{1,0:T(8,128)(2,1)} %all-gather.6.cloned.1.call-done) | copy-start | bytes 12582916
  236.5 4.5 %copy-start.3 = (bf16[128,4096]{1,0:T(8,128)(2,1)S(1)}, bf16[128,4096]{1,0:T(8,128)(2,1)}, u32[]{:S(2)}) copy-start(bf16[128,4096]{1,0:T(8,128)(2,1)} %all-gather.4.cloned.1.call-done) | copy-start | bytes 3145732
  236.5 5.5 %copy-start.1 = (bf16[128,4096]{1,0:T(8,128)(2,1)S(1)}, bf16[128,4096]{1,0:T(8,128)(2,1)}, u32[]{:S(2)}) copy-start(bf16[128,4096]{1,0:T(8,128)(2,1)} %param.5) | copy-start | bytes 3145732
Sparse Core Ops, SparseCore 0:
  62.8 22.7 all-gather.3
  89.0 61.7 all-gather.5
  154.1 60.5 all-gather.7

commit v2 on v1

v2 whole, which is shorter than its diff:
```python
import functools

import jax
import jax.numpy as jnp
from jax import lax
from jax.experimental import pallas as pl
from jax.experimental.pallas import tpu as pltpu
from jax.sharding import PartitionSpec as P

PLANE = ("fs", "tp")
MESH = pl.DeviceIdType.MESH


def contract_rows(left, right):
    return lax.dot_general(
        left, right, (((0,), (0,)), ((), ())), preferred_element_type=jnp.float32
    )


def contract_cols(left, right):
    return lax.dot_general(
        left, right, (((1,), (1,)), ((), ())), preferred_element_type=jnp.float32
    )


def greet(neighbours):
    barrier = pltpu.get_barrier_semaphore()
    for device in neighbours:
        pl.semaphore_signal(barrier, inc=1, device_id=device, device_id_type=MESH)
    pl.semaphore_wait(barrier, len(neighbours))


def gather_kernel(reps, x_ref, c_ref, all_x, all_c, send, recv, own_sem):
    z, y, t = lax.axis_index("rep"), lax.axis_index("fs"), lax.axis_index("tp")
    x, core = t // 2, t % 2
    half = (x + y) % 2
    mine = 2 * half + core
    across = 2 * (1 - half) + core
    up, down = (z + 1) % reps, (z + reps - 1) % reps
    to_up, to_down = (up, y, t), (down, y, t)
    x_near = (z, y, 2 * (x + 1 - 2 * (x % 2)) + core)
    y_near = (z, y + 1 - 2 * (y % 2), t)
    other = (z, y, 2 * x + 1 - core)
    greet((to_up, to_down, x_near, y_near, other))

    started = []

    def put(kind, step, src, dst, device):
        copy = pltpu.make_async_remote_copy(
            src_ref=src, dst_ref=dst, send_sem=send.at[kind, step],
            recv_sem=recv.at[kind, step], device_id=device, device_id_type=MESH,
        )
        copy.start()
        started.append(copy)
        return copy

    ring = [
        put(0, 0, x_ref.at[mine], all_x.at[z, mine], to_up),
        put(1, 0, c_ref.at[mine], all_c.at[z, mine], to_down),
    ]
    keep = [
        pltpu.make_async_copy(x_ref, all_x.at[z], own_sem.at[0]),
        pltpu.make_async_copy(c_ref, all_c.at[z], own_sem.at[1]),
    ]
    for copy in keep:
        copy.start()

    last = []

    def relay(sides, step, bx, bc):
        sides[0].wait_recv()
        last.append(put(6, step, all_x.at[bx, across], all_x.at[bx, across], other))
        sides[1].wait_recv()
        last.append(put(7, step, all_c.at[bc, across], all_c.at[bc, across], other))

    before = None
    for step in range(reps - 1):
        bx, bc = (z + reps - 1 - step) % reps, (z + 1 + step) % reps
        got_x, got_c = all_x.at[bx, mine], all_c.at[bc, mine]
        following = []
        ring[0].wait_recv()
        if step < reps - 2:
            following.append(put(0, step + 1, got_x, got_x, to_up))
        side_x = put(2, step, got_x, got_x, x_near)
        last.append(put(4, step, got_x, got_x, other))
        ring[1].wait_recv()
        if step < reps - 2:
            following.append(put(1, step + 1, got_c, got_c, to_down))
        side_c = put(3, step, got_c, got_c, y_near)
        last.append(put(5, step, got_c, got_c, other))
        if before is not None:
            relay(*before)
        before = ((side_x, side_c), step, bx, bc)
        ring = following
    relay(*before)
    for copy in last:
        copy.wait_recv()
    for copy in started:
        copy.wait_send()
    for copy in keep:
        copy.wait()


def gather(reps, inputs, cotangent):
    rows, width = inputs.shape
    quarter = (4, rows // 4, width)
    whole = jax.ShapeDtypeStruct((reps,) + quarter, inputs.dtype)
    vmem = pl.BlockSpec(memory_space=pltpu.VMEM)
    pair = pl.pallas_call(
        functools.partial(gather_kernel, reps),
        out_shape=(whole, whole),
        in_specs=[vmem, vmem],
        out_specs=(vmem, vmem),
        scratch_shapes=[
            pltpu.SemaphoreType.DMA((8, reps - 1)),
            pltpu.SemaphoreType.DMA((8, reps - 1)),
            pltpu.SemaphoreType.DMA((2,)),
        ],
        compiler_params=pltpu.CompilerParams(
            collective_id=0, has_side_effects=True, vmem_limit_bytes=60 * 2**20
        ),
        name="token_gather",
    )(inputs.reshape(quarter), cotangent.reshape(quarter))
    return [a.reshape(reps * rows, width) for a in pair]


def reduce_kernel(chips, across, terms, out, got, sums, landed, send, recv):
    z, y, t = lax.axis_index("rep"), lax.axis_index("fs"), lax.axis_index("tp")
    core = t % 2
    chip = y * across + t // 2
    other = (z, y, t + 1 - 2 * core)

    def peer(ahead):
        there = (chip + ahead) % chips
        return there, (z, there // across, 2 * (there % across) + core)

    greet([other] + [peer(ahead)[1] for ahead in range(1, chips)])

    def put(kind, slot, src, dst, device):
        copy = pltpu.make_async_remote_copy(
            src_ref=src, dst_ref=dst, send_sem=send.at[kind, slot],
            recv_sem=recv.at[kind, slot], device_id=device, device_id_type=MESH,
        )
        copy.start()
        return copy

    swaps = [put(0, j, terms.at[j, 1 - core], got.at[j], other) for j in range(chips)]
    for j in range(chips):
        swaps[j].wait_recv()
        pair = terms[j, core].astype(jnp.float32) + got[j].astype(jnp.float32)
        sums[j] = pair.astype(sums.dtype)
    spread = []
    for ahead in range(1, chips):
        there, device = peer(ahead)
        spread.append(put(1, ahead, sums.at[there], landed.at[ahead], device))
    total = terms[chip, core].astype(jnp.float32) + got[chip].astype(jnp.float32)
    for ahead in range(1, chips):
        spread[ahead - 1].wait_recv()
        total = total + landed[ahead].astype(jnp.float32)
    out[chip, core] = total.astype(out.dtype)
    done = out.at[chip, core]
    share = [put(2, ahead, done, done, peer(ahead)[1]) for ahead in range(1, chips)]
    relays = [put(3, 0, done, done, other)]
    for ahead in range(1, chips):
        share[ahead - 1].wait_recv()
        source = out.at[(chip + chips - ahead) % chips, core]
        relays.append(put(3, ahead, source, source, other))
    for copy in relays:
        copy.wait_recv()
    for copy in swaps + spread + share + relays:
        copy.wait_send()


def plane_sum(chips, across, terms):
    rows, width = terms.shape
    piece = (rows // (2 * chips), width)
    vmem = pl.BlockSpec(memory_space=pltpu.VMEM)
    total = pl.pallas_call(
        functools.partial(reduce_kernel, chips, across),
        out_shape=jax.ShapeDtypeStruct((chips, 2) + piece, terms.dtype),
        in_specs=[vmem],
        out_specs=vmem,
        scratch_shapes=[
            pltpu.VMEM((chips,) + piece, terms.dtype),
            pltpu.VMEM((chips,) + piece, terms.dtype),
            pltpu.VMEM((chips,) + piece, terms.dtype),
            pltpu.SemaphoreType.DMA((4, chips)),
            pltpu.SemaphoreType.DMA((4, chips)),
        ],
        compiler_params=pltpu.CompilerParams(
            collective_id=1, has_side_effects=True, vmem_limit_bytes=48 * 2**20
        ),
        name="plane_sum",
    )(terms.reshape((chips, 2) + piece))
    return total.reshape(rows, width)


def local(reps, chips, across, inputs, cotangent, w_gate, w_upward, w_down):
    rows, width = inputs.shape
    all_inputs, all_cotangent = gather(reps, inputs, cotangent)

    gate_pre = jnp.dot(all_inputs, w_gate, preferred_element_type=jnp.float32)
    up_pre = jnp.dot(all_inputs, w_upward, preferred_element_type=jnp.float32)
    sigmoid_gate = jax.nn.sigmoid(gate_pre)
    activated = gate_pre * sigmoid_gate
    hidden = (activated * up_pre).astype(jnp.bfloat16)
    hidden_grad = contract_cols(all_cotangent, w_down)
    gate_delta = (
        hidden_grad * up_pre * sigmoid_gate * (1.0 + gate_pre * (1.0 - sigmoid_gate))
    ).astype(jnp.bfloat16)
    up_delta = (hidden_grad * activated).astype(jnp.bfloat16)

    z = lax.axis_index("rep")
    own_gate = lax.dynamic_slice_in_dim(gate_delta, z * rows, rows, 0)
    own_up = lax.dynamic_slice_in_dim(up_delta, z * rows, rows, 0)
    terms = contract_cols(own_gate, w_gate) + contract_cols(own_up, w_upward)
    grad_input = plane_sum(chips, across, terms.astype(jnp.bfloat16))

    cols = width // reps
    input_cols = lax.dynamic_slice_in_dim(all_inputs, z * cols, cols, 1)
    cotangent_cols = lax.dynamic_slice_in_dim(all_cotangent, z * cols, cols, 1)
    grad_gate = contract_rows(input_cols, gate_delta)
    grad_upward = contract_rows(input_cols, up_delta)
    grad_down = contract_rows(hidden, cotangent_cols)
    return (grad_input, grad_gate, grad_upward, grad_down)


def solution(mesh):
    across = mesh.shape["tp"] // 2
    chips = mesh.shape["fs"] * across
    in_specs = (
        P("rep", None),
        P("rep", None),
        P(None, PLANE),
        P(None, PLANE),
        P(PLANE, None),
    )
    out_specs = (
        P("rep", None),
        P("rep", PLANE),
        P("rep", PLANE),
        P(PLANE, "rep"),
    )
    body = functools.partial(local, mesh.shape["rep"], chips, across)
    return jax.shard_map(body, mesh=mesh, in_specs=in_specs, out_specs=out_specs, check_vma=False)
```

time: 249 us -> 142 us (0.57)
  waiting for transfers between devices: 125 us -> 0 us
  Pallas kernels: 0 us -> 75.4 us
  blocking collectives: 20.3 us -> 0 us
  matrix products: 84.8 us -> 65.1 us
  between operations: 13.8 us -> 0.78 us
    all_gather x3 -> x0, waiting for transfers between devices: 125 us -> none  [the longest x2 105 us: local(): lax.all_gather(a, everyone, axis=0, tiled=True)]
    pallas_call x0 -> x2, Pallas kernels: none -> 75.4 us  [the longest x1 55.2 us: gather(): pl.pallas_call(functools.partial(gather_kernel, reps), out_shape=(whole,...]
    all_to_all x1 -> x0, blocking collectives: 20.3 us -> none  [local(): terms = lax.all_to_all(terms.reshape(planes, share, width), PLANE, 0, 0)]
    dot_general x4 -> x3, matrix products: 43 us -> 26.8 us  [contract_cols(): lax.dot_general(left, right, (((1,), (1,)), ((), ())), preferred_element_...]
    dot_general x3 -> x2, matrix products: 27 us -> 20.3 us  [the longest x1 12.1 us: local(): gate_pre = jnp.dot(all_inputs, w_gate, preferred_element_type=jnp.float32)]
    dot_general x3, matrix products: 14.8 us -> 17.9 us  [contract_rows(): lax.dot_general(left, right, (((0,), (0,)), ((), ())), preferred_element_...]
  transfers between devices with their start and end apart: 3 -> 0, of which waited for: 3 -> 0; matrix products, arithmetic and copies ran while one was open for 11% -> 0% of each run, Pallas kernels for 0% -> 0%
where the time goes in v2:
time: 142 us
  Pallas kernels  75.4 us (53%)
  matrix products  65.1 us (46%)
    pallas_call x1, Pallas kernels, gather(): pl.pallas_call(functools.partial(gather_kernel, reps), out_shape=(whole,...  55.2 us
    dot_general x3, matrix products, contract_cols(): lax.dot_general(left, right, (((1,), (1,)), ((), ())), preferred_element_...  26.8 us
    pallas_call x1, Pallas kernels, plane_sum(): pl.pallas_call(functools.partial(reduce_kernel, chips, across), out_shape...  20.1 us
    dot_general x3, matrix products, contract_rows(): lax.dot_general(left, right, (((0,), (0,)), ((), ())), preferred_element_...  17.9 us
    dot_general x1, matrix products, local(): gate_pre = jnp.dot(all_inputs, w_gate, preferred_element_type=jnp.float32)  12.1 us
    dot_general x1, matrix products, local(): up_pre = jnp.dot(all_inputs, w_upward, preferred_element_type=jnp.float32)  8.26 us

profile of v2, /device:TPU:0, one launch (start us, length us, event | category | flops | bytes accessed | tf_op | source)
XLA Modules:
  0.0 142.3 jit_solution(7572952296496078483)
XLA Ops:
  0.6 0.0 slice-start
  0.7 55.2 %token_gather.1 = (bf16[4,4,32,4096]{3,2,1,0:T(8,128)(2,1)}, bf16[4,4,32,4096]{3,2,1,0:T(8,128)(2,1)}) custom-call(bf16[4,32,4096]{2,1,0:T(8,128)(2,1)} %bitcast.22, bf16[4,32,4096]{2,1,0:T(8,128)(2,1)} %bitcast.23), custom_call_target="tpu_custom_call" | custom-call | tf_op jit(solution)/shard_map/token_gather/pallas_call | solution.py:109
  55.9 0.0 slice-start.1
  55.9 0.0 slice-start.2
  55.9 0.0 copy-start.1
  55.9 12.1 %fusion.19 = f32[512,1408]{1,0:T(8,128)} fusion(bf16[512,4096]{1,0:T(8,128)(2,1)} %bitcast.24, bf16[4096,1408]{1,0:T(8,128)(2,1)} %param.7), kind=kOutput, calls=%fused_computation.23 | convolution fusion | flops 5905580032 | bytes 18612224 | tf_op jit(solution)/shard_map/dot_general | solution.py:202
  68.0 0.0 slice-done
  68.0 0.0 slice-done.1
  68.0 0.0 slice-done.2
  68.0 0.0 copy-done.1
  68.0 8.3 %fusion.18 = f32[512,1408]{1,0:T(8,128)} fusion(bf16[512,4096]{1,0:T(8,128)(2,1)S(1)} %bitcast.27, bf16[4096,1408]{1,0:T(8,128)(2,1)S(1)} %bitcast.19), kind=kOutput, calls=%fused_computation.22 | convolution fusion | flops 5905580032 | bytes 18612224 | tf_op jit(solution)/shard_map/dot_general | solution.py:203
  76.3 14.8 %multiply_convert_fusion.1 = (bf16[512,1408]{1,0:T(8,128)(2,1)S(1)}, bf16[512,1408]{1,0:T(8,128)(2,1)}) fusion(f32[512,1408]{1,0:T(8,128)} %fusion.19, f32[512,1408]{1,0:T(8,128)} %fusion.18, bf16[512,4096]{1,0:T(8,128)(2,1)} %bitcast.28, bf16[1408,4096]{1,0:T(8,128)(2,1)} %param.9), kind=kOutput, calls=%fused_computation.3 | convolution fusion | flops 5914951680 | bytes 24379392 | tf_op jit(solution)/shard_map/dot_general | solution.py:21
  91.0 0.0 copy-done.2
  91.1 0.0 slice-start.4
  91.1 6.6 %fusion.2 = f32[1408,1024]{1,0:T(8,128)} fusion(f32[512,1408]{1,0:T(8,128)} %fusion.18, bf16[512,4096]{1,0:T(8,128)(2,1)} %bitcast.29, s32[]{:T(128)S(6)} %select_n.9, f32[512,1408]{1,0:T(8,128)S(1)} %copy-done.2), kind=kOutput, calls=%fused_computation.7 | convolution fusion | flops 1480720384 | bytes 12582916 | tf_op jit(solution)/shard_map/dot_general | solution.py:15
  97.6 8.3 %fusion.10 = f32[128,4096]{1,0:T(8,128)S(1)} fusion(bf16[4096,1408]{1,0:T(8,128)(2,1)} %param.7, bf16[512,1408]{1,0:T(8,128)(2,1)} %get-tuple-element.9, s32[]{:T(128)S(6)} %select_n.8), kind=kOutput, calls=%fused_computation.14 | convolution fusion | flops 1476395008 | bytes 13991940 | tf_op jit(solution)/shard_map/dot_general | solution.py:21
  106.0 0.0 slice-done.3
  106.0 0.0 slice-done.4
  106.0 3.8 %fusion = bf16[128,4096]{1,0:T(8,128)(2,1)S(1)} fusion(f32[128,4096]{1,0:T(8,128)S(1)} %fusion.10, bf16[4096,1408]{1,0:T(8,128)(2,1)S(1)} %bitcast.21, bf16[512,1408]{1,0:T(8,128)(2,1)S(1)} %get-tuple-element.8, s32[]{:T(128)S(6)} %select_n.8), kind=kOutput, calls=%fused_computation.1 | convolution fusion | flops 1477443584 | bytes 15040516 | tf_op jit(solution)/shard_map/dot_general | solution.py:21
  109.8 20.1 %plane_sum.1 = bf16[4,2,16,4096]{3,2,1,0:T(8,128)(2,1)S(1)} custom-call(bf16[4,2,16,4096]{3,2,1,0:T(8,128)(2,1)S(1)} %bitcast.16), custom_call_target="tpu_custom_call" | custom-call | tf_op jit(solution)/shard_map/plane_sum/pallas_call | solution.py:178
  129.9 0.0 copy-start
  129.9 5.7 %fusion.4 = f32[1024,1408]{1,0:T(8,128)} fusion(bf16[512,1408]{1,0:T(8,128)(2,1)S(1)} %get-tuple-element.8, bf16[512,4096]{1,0:T(8,128)(2,1)} %bitcast.25, s32[]{:T(128)S(6)} %select_n.9), kind=kOutput, calls=%fused_computation.9 | convolution fusion | flops 1476395008 | bytes 8257540 | tf_op jit(solution)/shard_map/dot_general | solution.py:15
  135.7 5.6 %fusion.6 = f32[1024,1408]{1,0:T(8,128)} fusion(bf16[512,1408]{1,0:T(8,128)(2,1)S(1)} %copy-done, bf16[512,4096]{1,0:T(8,128)(2,1)} %bitcast.26, s32[]{:T(128)S(6)} %select_n.9), kind=kOutput, calls=%fused_computation.11 | convolution fusion | flops 1476395008 | bytes 8257540 | tf_op jit(solution)/shard_map/dot_general | solution.py:15
  141.3 1.0 copy.10
  (7 shorter events, 0.0 us)
Async XLA Ops:
  0.6 67.4 %slice-start = ((s8[11534336]{0:T(1024)(128)(4,1)}), s8[3145728]{0:T(1024)(128)(4,1)S(1)}, s32[]{:S(2)}) async-start(s8[11534336]{0:T(1024)(128)(4,1)} %bitcast.18), calls=%async_computation | async-start | bytes 6291456
  55.9 12.1 %slice-start.1 = ((s8[11534336]{0:T(1024)(128)(4,1)}), s8[4194304]{0:T(1024)(128)(4,1)S(1)}, s32[]{:S(2)}) async-start(s8[11534336]{0:T(1024)(128)(4,1)} %bitcast.18), calls=%async_computation.1 | async-start | bytes 8388608
  55.9 12.1 %slice-start.2 = ((s8[11534336]{0:T(1024)(128)(4,1)}), s8[4194304]{0:T(1024)(128)(4,1)S(1)}, s32[]{:S(2)}) async-start(s8[11534336]{0:T(1024)(128)(4,1)} %bitcast.18), calls=%async_computation.2 | async-start | bytes 8388608
  55.9 12.1 %copy-start.1 = (bf16[4,4,32,4096]{3,2,1,0:T(8,128)(2,1)S(1)}, bf16[4,4,32,4096]{3,2,1,0:T(8,128)(2,1)}, u32[]{:S(2)}) copy-start(bf16[4,4,32,4096]{3,2,1,0:T(8,128)(2,1)} %get-tuple-element.7) | copy-start | bytes 12582916
  76.3 14.8 %copy-start.2 = (f32[512,1408]{1,0:T(8,128)S(1)}, f32[512,1408]{1,0:T(8,128)}, u32[]{:S(2)}) copy-start(f32[512,1408]{1,0:T(8,128)} %fusion.19) | copy-start | bytes 8650756
  91.1 14.9 %slice-start.3 = ((s8[11534336]{0:T(1024)(128)(4,1)}), s8[4194304]{0:T(1024)(128)(4,1)S(1)}, s32[]{:S(2)}) async-start(s8[11534336]{0:T(1024)(128)(4,1)} %bitcast.20), calls=%async_computation.3 | async-start | bytes 8388608
  91.1 14.9 %slice-start.4 = ((s8[11534336]{0:T(1024)(128)(4,1)}), s8[4194304]{0:T(1024)(128)(4,1)S(1)}, s32[]{:S(2)}) async-start(s8[11534336]{0:T(1024)(128)(4,1)} %bitcast.20), calls=%async_computation.4 | async-start | bytes 8388608
  97.6 8.3 %slice-start.5 = ((s8[11534336]{0:T(1024)(128)(4,1)}), s8[3145728]{0:T(1024)(128)(4,1)S(1)}, s32[]{:S(2)}) async-start(s8[11534336]{0:T(1024)(128)(4,1)} %bitcast.20), calls=%async_computation.5 | async-start | bytes 6291456
  129.9 5.7 %copy-start = (bf16[512,1408]{1,0:T(8,128)(2,1)S(1)}, bf16[512,1408]{1,0:T(8,128)(2,1)}, u32[]{:S(2)}) copy-start(bf16[512,1408]{1,0:T(8,128)(2,1)} %get-tuple-element.9) | copy-start | bytes 4325380
